TPU v7x, 32 devices: a whole 2x2x4 slice. The times are simulated.
32 devices in a mesh: sp: 8 (over z, x), tp: 4 (over y, core).
Axes of the slice: x: 2, y: 2, z: 4, core: 2. Of those that a mesh axis runs over, the one named last changes fastest.
Arguments:
- residual: bfloat16 [4096, 2048], P('sp'), may hold values from -80 to 80
- queries: bfloat16 [4096, 1024], P('sp', 'tp'), may hold values from -260 to 260
- keys: bfloat16 [4096, 512], P('sp', 'tp'), may hold values from -7 to 7
- values: bfloat16 [4096, 512], P('sp', 'tp'), may hold values from -12 to 12
- documents: int32 [4096], P('sp'), may hold values from 0 to 3, never falling along the last dimension, each value on 1 to 3072 neighbouring positions
- sinks: float32 [16], P('tp'), may hold values from 1 to 6
- out_weight: bfloat16 [1024, 2048], P('tp'), may hold values from -0.5 to 0.5
- norm_gain: float32 [2048], replicated, may hold values from 0.1 to 1.9
- gate_weight: bfloat16 [2048, 5632], P('sp', 'tp'), may hold values from -0.125 to 0.125
- up_weight: bfloat16 [2048, 5632], P('sp', 'tp'), may hold values from -0.125 to 0.125
- down_weight: bfloat16 [2048, 5632], P('sp', 'tp'), may hold values from -0.078125 to 0.078125
Outputs:
- mixed: bfloat16 [4096, 2048], P('sp', 'tp')
Inputs may be any that keep to these rules, and one draw needn't show every extreme that they name: `documents`: document numbers never fall along the positions; a document holds at most 3072 positions.
All inputs are finite; a program needn't handle non-finite values.
Results may differ from a plain program's by a relative error of at most 0.01.
Values may be sent and summed in bfloat16 or wider, within the bound.
A program may use at most 64 MiB of HBM per device.

v0:
```python
import jax
import jax.numpy as jnp
from jax import lax
from jax.sharding import PartitionSpec as P

HEAD_DIM = 64
WINDOW = 128
GROUP = 2


neg_big = -1e30
norm_eps = 1e-05


def from_behind(shard, axis, by):
    length = lax.axis_size(axis)
    pairs = [(i, i + by) for i in range(length) if 0 <= i + by < length]
    return lax.ppermute(shard, axis, pairs)


def attend(queries, keys, values, documents, sinks, tail_keys, tail_values, tail_docs, offset):
    rows_here = queries.shape[0]
    block_count = rows_here // WINDOW
    kv_here = keys.shape[1] // HEAD_DIM
    q_blocks = queries.reshape(block_count, WINDOW, kv_here, GROUP, HEAD_DIM)
    k_blocks = keys.reshape(block_count, WINDOW, kv_here, HEAD_DIM)
    v_blocks = values.reshape(block_count, WINDOW, kv_here, HEAD_DIM)
    k_prev = jnp.concatenate(
        [tail_keys.reshape(1, WINDOW, kv_here, HEAD_DIM), k_blocks[:-1]], axis=0
    )
    v_prev = jnp.concatenate(
        [tail_values.reshape(1, WINDOW, kv_here, HEAD_DIM), v_blocks[:-1]], axis=0
    )
    k_band = jnp.concatenate([k_prev, k_blocks], axis=1)
    v_band = jnp.concatenate([v_prev, v_blocks], axis=1)
    doc_own = documents.astype(jnp.float32).reshape(block_count, WINDOW)
    doc_prev = jnp.concatenate(
        [tail_docs.astype(jnp.float32).reshape(1, WINDOW), doc_own[:-1]], axis=0
    )
    doc_band = jnp.concatenate([doc_prev, doc_own], axis=1)
    row_idx = jnp.arange(WINDOW, dtype=jnp.int32)
    col_idx = jnp.arange(2 * WINDOW, dtype=jnp.int32)
    first = offset + jnp.arange(block_count, dtype=jnp.int32) * WINDOW
    q_pos = first[:, None] + row_idx[None, :]
    k_pos = first[:, None] - WINDOW + col_idx[None, :]
    distance = q_pos[:, :, None] - k_pos[:, None, :]
    visible = (
        (distance >= 0)
        & (distance < WINDOW)
        & (k_pos[:, None, :] >= 0)
        & (doc_own[:, :, None] == doc_band[:, None, :])
    )
    scores = jnp.einsum(
        "nikgd,njkd->nkgij", q_blocks, k_band, preferred_element_type=jnp.float32
    ) * HEAD_DIM ** (-0.5)
    scores = jnp.where(visible[:, None, None], scores, neg_big)
    sink_logit = sinks.reshape(1, kv_here, GROUP, 1, 1)
    row_max = jnp.maximum(scores.max(-1, keepdims=True), sink_logit)
    expo = jnp.where(visible[:, None, None], jnp.exp(scores - row_max), 0.0)
    denom_sum = expo.sum(-1, keepdims=True) + jnp.exp(sink_logit - row_max)
    weights = (expo / denom_sum).astype(jnp.bfloat16)
    mixed = jnp.einsum("nkgij,njkd->nikgd", weights, v_band, preferred_element_type=jnp.float32)
    return mixed.reshape(rows_here, kv_here * GROUP * HEAD_DIM).astype(jnp.bfloat16)


def on_device(
    residual,
    queries,
    keys,
    values,
    documents,
    sinks,
    out_weight,
    norm_gain,
    gate_weight,
    up_weight,
    down_weight,
):
    rows_here = queries.shape[0]
    offset = lax.axis_index("sp") * rows_here
    doc_tail = documents[rows_here - WINDOW :].astype(jnp.bfloat16)
    tail_keys, tail_values, tail_docs = from_behind(
        (keys[rows_here - WINDOW :], values[rows_here - WINDOW :], doc_tail), "sp", 1
    )
    attended = attend(
        queries, keys, values, documents, sinks, tail_keys, tail_values, tail_docs, offset
    )
    model_width = residual.shape[1]
    col_count = model_width // lax.axis_size("tp")
    col_first = lax.axis_index("tp") * col_count
    full_term = jnp.dot(attended, out_weight, preferred_element_type=jnp.float32)
    projected = lax.psum(full_term.astype(jnp.bfloat16), "tp").astype(jnp.float32)
    after_full = (residual.astype(jnp.float32) + projected).astype(jnp.bfloat16)
    after_f = after_full.astype(jnp.float32)
    inv_rms = lax.rsqrt(jnp.mean(after_f * after_f, axis=1, keepdims=True) + norm_eps)
    normed = (after_f * inv_rms * norm_gain[None, :]).astype(jnp.bfloat16)
    after = lax.dynamic_slice_in_dim(after_full, col_first, col_count, 1)
    gate_act = jnp.dot(
        normed,
        lax.all_gather(gate_weight, "sp", axis=0, tiled=True),
        preferred_element_type=jnp.float32,
    )
    up_act = jnp.dot(
        normed,
        lax.all_gather(up_weight, "sp", axis=0, tiled=True),
        preferred_element_type=jnp.float32,
    )
    down_full = lax.all_gather(down_weight, "sp", axis=0, tiled=True)
    hidden = (jax.nn.silu(gate_act) * up_act).astype(jnp.bfloat16)
    summed = lax.psum_scatter(
        lax.dot_general(
            down_full, hidden, (((1,), (1,)), ((), ())), preferred_element_type=jnp.float32
        ).astype(jnp.bfloat16),
        "tp",
        scatter_dimension=0,
        tiled=True,
    ).astype(jnp.float32)
    return (after.astype(jnp.float32) + summed.T).astype(jnp.bfloat16)


def solution(mesh):
    return jax.shard_map(
        on_device,
        mesh=mesh,
        in_specs=(
            P("sp", None),
            P("sp", "tp"),
            P("sp", "tp"),
            P("sp", "tp"),
            P("sp"),
            P("tp"),
            P("tp", None),
            P(),
            P("sp", "tp"),
            P("sp", "tp"),
            P("sp", "tp"),
        ),
        out_specs=P("sp", "tp"),
        check_vma=False,
    )
```

profile of v0, /device:TPU:0, one launch (start us, length us, event | category | flops | bytes accessed | tf_op | source)
XLA Modules:
  0.0 367.5 jit_solution(8054649888373592953)
XLA Ops:
  7.4 0.0 copy-start
  7.4 0.0 slice-start
  7.4 0.0 slice-start.1
  7.4 0.0 copy-start.3
  7.4 0.0 all-reduce.2.cloned.1.call-start
  7.4 0.8 fusion.34
  8.2 4.9 %collective-permute-start.1 = (bf16[128]{0:T(256)(128)(2,1)S(1)}, bf16[128]{0:T(256)(128)(2,1)S(1)}, u32[]{:S(2)}, u32[]{:S(2)}) collective-permute-start(bf16[128]{0:T(256)(128)(2,1)S(1)} %slice.39), channel_id=1, source_target_pairs={{0,4},{4,8},{8,12},{12,16},{16,20},{20,24},{24,28},{1,5},{5,9},{9,... | collective-permute-start | bytes 776 | tf_op jit(solution)/shard_map/ppermute | solution.py:18
  13.1 0.8 slice.42
  13.9 3.4 collective-permute-start.2
  17.3 1.4 slice.36
  18.7 4.0 %collective-permute-start = (bf16[128,128]{1,0:T(8,128)(2,1)}, bf16[128,128]{1,0:T(8,128)(2,1)}, u32[]{:S(2)}, u32[]{:S(2)}) collective-permute-start(bf16[128,128]{1,0:T(8,128)(2,1)} %slice.36), channel_id=1, source_target_pairs={{0,4},{4,8},{8,12},{12,16},{16,20},{20,24},{24,28},{1,5},{5,9},{9,... | collective-permute-start | bytes 98312 | tf_op jit(solution)/shard_map/ppermute | solution.py:18
  22.7 0.1 iota_add_fusion
  22.7 0.1 broadcast_compare_fusion
  22.8 1.0 reshape.148
  23.9 1.0 reshape.146
  24.9 0.1 iota_add_fusion.1
  25.0 2.0 reshape.149
  27.0 0.0 slice-done
  27.0 0.1 reshape.147
  27.1 0.8 copy.23
  27.9 0.1 copy.25
  28.1 0.0 copy-done.3
  28.1 0.1 max.18
  28.1 0.0 slice-done.1
  28.2 0.1 reshape.145
  28.3 0.8 copy.18
  29.1 0.1 copy.20
  29.2 0.0 collective-permute-done.1
  29.2 0.6 fusion.17
  29.8 0.0 collective-permute-done.2
  29.8 0.7 copy.21
  30.5 1.6 fusion.5
  32.2 0.0 copy-start.1
  32.2 0.1 broadcast_maximum_fusion
  32.3 0.5 fusion.6
  32.8 0.1 exponential_add_fusion
  32.9 0.0 collective-permute-done
  32.9 0.9 copy.16
  33.8 0.0 copy-done.1
  33.8 0.7 fusion.7
  34.5 0.2 copy.29
  34.7 0.0 copy-done
  34.7 2.1 convolution_convert_fusion
  36.8 0.0 all-reduce.2.cloned.1.call-update
  36.8 0.0 all-gather.4.cloned.1.call-start
  36.9 0.5 all-gather.4.cloned.1.call-update
  37.4 0.0 all-gather.6.cloned.1.call-start
  37.4 0.5 all-gather.6.cloned.1.call-update
  38.0 0.0 all-gather.8.cloned.1.call-start
  38.0 0.5 all-gather.8.cloned.1.call-update
  38.6 0.0 copy-start.2
  38.6 0.2 reduce-scatter.2.cloned.1.call-start
  38.8 48.3 %all-reduce.2.cloned.1.call-done = bf16[512,2048]{1,0:T(8,128)(2,1)} async-done(((bf16[512,2048]{1,0:T(8,128)(2,1)}), bf16[512,2048]{1,0:T(8,128)(2,1)}) %all-reduce.2.cloned.1.call-update) | async-done | bytes 2097168 | tf_op jit(solution)/shard_map/psum | solution.py:92
  87.1 3.2 fusion
  90.3 40.1 %all-gather.4.cloned.1.call-done = bf16[2048,1408]{1,0:T(8,128)(2,1)} async-done(((bf16[256,1408]{1,0:T(8,128)(2,1)}), bf16[2048,1408]{1,0:T(8,128)(2,1)}) %all-gather.4.cloned.1.call-update) | async-done | bytes 5767184 | tf_op jit(solution)/shard_map/all_gather | solution.py:100
  130.4 0.0 copy-done.2
  130.4 7.6 %fusion.11 = f32[512,1408]{1,0:T(8,128)} fusion(bf16[2048,1408]{1,0:T(8,128)(2,1)} %all-gather.4.cloned.1.call-done, bf16[512,2048]{1,0:T(8,128)(2,1)S(1)} %get-tuple-element.6, f32[2048]{0:T(1024)S(1)} %copy-done.2, f32[512]{0:T(512)S(1)} %add_rsqrt_fusion), kind=kOutput, calls=%fused_computation.22 | convolution fusion | flops 2956984320 | bytes 10758144 | tf_op jit(solution)/shard_map/dot_general | solution.py:98
  138.0 84.7 %all-gather.6.cloned.1.call-done = bf16[2048,1408]{1,0:T(8,128)(2,1)} async-done(((bf16[256,1408]{1,0:T(8,128)(2,1)}), bf16[2048,1408]{1,0:T(8,128)(2,1)}) %all-gather.6.cloned.1.call-update) | async-done | bytes 5767184 | tf_op jit(solution)/shard_map/all_gather | solution.py:105
  222.7 92.4 %all-gather.8.cloned.1.call-done = bf16[2048,1408]{1,0:T(8,128)(2,1)} async-done(((bf16[256,1408]{1,0:T(8,128)(2,1)}), bf16[2048,1408]{1,0:T(8,128)(2,1)}) %all-gather.8.cloned.1.call-update) | async-done | bytes 5767184 | tf_op jit(solution)/shard_map/all_gather | solution.py:108
  315.1 13.4 %fusion.4 = bf16[2048,512]{0,1:T(8,128)(2,1)} fusion(bf16[2048,1408]{1,0:T(8,128)(2,1)} %all-gather.8.cloned.1.call-done, bf16[2048,1408]{1,0:T(8,128)(2,1)} %all-gather.6.cloned.1.call-done, f32[512,1408]{1,0:T(8,128)} %fusion.11, bf16[512,2048]{1,0:T(8,128)(2,1)S(1)} %get-tuple-element.6, f32[2048]{0:T(1024)S(1)} %copy-done.2, f32[512]{0:T(512)S(1)} %add_rsqrt_fusion), kind=kOutput, calls=%fused_computation.10 | convolution fusion | flops 5915148288 | bytes 18622464 | tf_op jit(solution)/shard_map/dot_general | solution.py:111
  328.5 0.0 reduce-scatter.2.cloned.1.call-update
  328.5 29.5 %reduce-scatter.2.cloned.1.call-done = bf16[512,512]{0,1:T(8,128)(2,1)} async-done(((bf16[2048,512]{0,1:T(8,128)(2,1)}), bf16[512,512]{0,1:T(8,128)(2,1)}) %reduce-scatter.2.cloned.1.call-update) | async-done | bytes 524304 | tf_op jit(solution)/shard_map/reduce_scatter | solution.py:110
  358.0 2.0 fusion.8
  (6 shorter events, 0.0 us)
Async XLA Ops:
  7.4 27.3 %copy-start = (bf16[256,2048]{1,0:T(8,128)(2,1)S(1)}, bf16[256,2048]{1,0:T(8,128)(2,1)}, u32[]{:S(2)}) copy-start(bf16[256,2048]{1,0:T(8,128)(2,1)} %param.17) | copy-start | bytes 3145732
  7.4 19.6 %slice-start = ((bf16[512,128]{1,0:T(8,128)(2,1)}), bf16[384,128]{1,0:T(8,128)(2,1)S(1)}, s32[]{:S(2)}) async-start(bf16[512,128]{1,0:T(8,128)(2,1)} %param.13), calls=%async_computation.6 | async-start | bytes 196608 | tf_op jit(solution)/shard_map/slice | solution.py:29
  7.4 20.8 %slice-start.1 = ((bf16[512,128]{1,0:T(8,128)(2,1)}), bf16[384,128]{1,0:T(8,128)(2,1)S(1)}, s32[]{:S(2)}) async-start(bf16[512,128]{1,0:T(8,128)(2,1)} %param.14), calls=%async_computation.7 | async-start | bytes 196608 | tf_op jit(solution)/shard_map/slice | solution.py:32
  7.4 20.7 %copy-start.3 = (f32[4]{0:T(128)S(1)}, f32[4]{0:T(128)}, u32[]{:S(2)}) copy-start(f32[4]{0:T(128)} %param.16) | copy-start | bytes 52
  7.4 79.7 %all-reduce.2.cloned.1.call-start = ((), (), s32[]{:S(2)}) async-start(), calls=%async_computation.1 | async-start | bytes 4194304 | tf_op jit(solution)/shard_map/psum | solution.py:92
  8.2 21.0 %collective-permute-start.1 = (bf16[128]{0:T(256)(128)(2,1)S(1)}, bf16[128]{0:T(256)(128)(2,1)S(1)}, u32[]{:S(2)}, u32[]{:S(2)}) collective-permute-start(bf16[128]{0:T(256)(128)(2,1)S(1)} %slice.39), channel_id=1, source_target_pairs={{0,4},{4,8},{8,12},{12,16},{16,20},{20,24},{24,28},{1,5},{5,9},{9,... | collective-permute-start | bytes 776 | tf_op jit(solution)/shard_map/ppermute | solution.py:18
  13.9 16.0 %collective-permute-start.2 = (bf16[128,128]{1,0:T(8,128)(2,1)S(1)}, bf16[128,128]{1,0:T(8,128)(2,1)S(1)}, u32[]{:S(2)}, u32[]{:S(2)}) collective-permute-start(bf16[128,128]{1,0:T(8,128)(2,1)S(1)} %slice.42), channel_id=1, source_target_pairs={{0,4},{4,8},{8,12},{12,16},{16,20},{20,24},{24,28},{1,5},{5,9},{9,... | collective-permute-start | bytes 98312 | tf_op jit(solution)/shard_map/ppermute | solution.py:18
  18.7 14.2 %collective-permute-start = (bf16[128,128]{1,0:T(8,128)(2,1)}, bf16[128,128]{1,0:T(8,128)(2,1)}, u32[]{:S(2)}, u32[]{:S(2)}) collective-permute-start(bf16[128,128]{1,0:T(8,128)(2,1)} %slice.36), channel_id=1, source_target_pairs={{0,4},{4,8},{8,12},{12,16},{16,20},{20,24},{24,28},{1,5},{5,9},{9,... | collective-permute-start | bytes 98312 | tf_op jit(solution)/shard_map/ppermute | solution.py:18
  32.2 1.6 copy-start.1
  36.8 93.5 %all-gather.4.cloned.1.call-start = ((), (), s32[]{:S(2)}) async-start(), calls=%async_computation.2 | async-start | bytes 6488064 | tf_op jit(solution)/shard_map/all_gather | solution.py:100
  37.4 185.3 %all-gather.6.cloned.1.call-start = ((), (), s32[]{:S(2)}) async-start(), calls=%async_computation.3 | async-start | bytes 6488064 | tf_op jit(solution)/shard_map/all_gather | solution.py:105
  38.0 277.1 %all-gather.8.cloned.1.call-start = ((), (), s32[]{:S(2)}) async-start(), calls=%async_computation.4 | async-start | bytes 6488064 | tf_op jit(solution)/shard_map/all_gather | solution.py:108
  38.6 91.8 %copy-start.2 = (f32[2048]{0:T(1024)S(1)}, f32[2048]{0:T(1024)}, u32[]{:S(2)}) copy-start(f32[2048]{0:T(1024)} %param.18) | copy-start | bytes 24580
  38.6 319.4 %reduce-scatter.2.cloned.1.call-start = ((), (), s32[]{:S(2)}) async-start(), calls=%async_computation.5 | async-start | bytes 2621440 | tf_op jit(solution)/shard_map/reduce_scatter | solution.py:110
Sparse Core Ops, SparseCore 0:
  36.9 50.1 all-reduce.1
  328.6 29.2 reduce-scatter.1
Sparse Core Ops, SparseCore 1:
  39.5 90.8 all-gather.3
  132.4 90.2 all-gather.5
  224.8 90.2 all-gather.7
where the time goes:
time: 368 us
  waiting for transfers between devices  296 us (80%)
  matrix products  25.5 us (7%)
  between operations  15.2 us (4%)
  starting transfers between devices  12.7 us (3%)
  local copies, waits for them, and re-layouts  10.2 us (3%)
  other arithmetic  7.52 us (2%)
    all_gather x1, waiting for transfers between devices, on_device(): down_full = lax.all_gather(down_weight, 'sp', axis=0, tiled=True)  92.4 us
    all_gather x1, waiting for transfers between devices, on_device(): lax.all_gather(up_weight, 'sp', axis=0, tiled=True)  84.7 us
    psum x1, waiting for transfers between devices, on_device(): lax.psum(full_term.astype(jnp.bfloat16), 'tp').astype(jnp.float32)  48.3 us
    all_gather x1, waiting for transfers between devices, on_device(): lax.all_gather(gate_weight, 'sp', axis=0, tiled=True)  40.1 us
    reduce_scatter x1, waiting for transfers between devices, on_device(): lax.psum_scatter(lax.dot_general(down_full, hidden, (((1,), (1,)), ((), (...  29.5 us
    dot_general x1, matrix products, on_device(): lax.dot_general(down_full, hidden, (((1,), (1,)), ((), ())), preferred_el...  13.4 us
    ppermute x3, starting transfers between devices, from_behind(): return lax.ppermute(shard, axis, pairs)  12.3 us
    dot_general x1, matrix products, on_device(): jnp.dot(normed, lax.all_gather(gate_weight, 'sp', axis=0, tiled=True), pr...  7.64 us
  transfers between devices with their start and end apart: 8, of which 5 were waited for; matrix products, arithmetic and copies ran while one was open for 6% of the time, Pallas kernels for 0%

commit v1 on v0

--- a/solution.py
+++ b/solution.py
@@ -1,6 +1,10 @@
+import functools
+
 import jax
 import jax.numpy as jnp
 from jax import lax
+from jax.experimental import pallas as pl
+from jax.experimental.pallas import tpu as pltpu
 from jax.sharding import PartitionSpec as P
 
 HEAD_DIM = 64
@@ -118,9 +122,375 @@
     return (after.astype(jnp.float32) + summed.T).astype(jnp.bfloat16)
 
 
+MESH = pl.DeviceIdType.MESH
+NT = (((1,), (1,)), ((), ()))
+
+
+def dot(a, b, dims=(((1,), (0,)), ((), ()))):
+    return lax.dot_general(a, b, dims, preferred_element_type=jnp.float32)
+
+
+def kernel(
+    S, T,
+    res_hbm, q_ref, k_ref, v_ref, doc_ref, sink_ref, ow_hbm, gain_ref, g_hbm, u_hbm, d_hbm,
+    out_ref,
+    G, kx, vx, dx, att, res_v, ow_v, psend, precv, after, normed, ga, ua, hidden, dsend, drecv,
+    w_send, w_recv, tail_send, tail_recv, loc, p_send, p_recv, a_send, a_recv, d_send, d_recv,
+):
+    s = lax.axis_index("sp")
+    t = lax.axis_index("tp")
+    R = q_ref.shape[0]
+    D = gain_ref.shape[1]
+    C = D // T
+    K = D // S
+    F = g_hbm.shape[1]
+    HK = K // 2
+    PER = C // K
+    z, x = s // 2, s % 2
+    zp = ((z + 1) % 4) * 2 + x
+    zm = ((z + 3) % 4) * 2 + x
+    z2 = ((z + 2) % 4) * 2 + x
+    xp = z * 2 + (1 - x)
+    zp_x = ((z + 1) % 4) * 2 + (1 - x)
+    zm_x = ((z + 3) % 4) * 2 + (1 - x)
+    z2_x = ((z + 2) % 4) * 2 + (1 - x)
+    after_s = (s + 1) % S
+    before_s = (s + S - 1) % S
+
+    weights = (g_hbm, u_hbm, d_hbm)
+    local = [
+        pltpu.make_async_copy(weights[m], G.at[m, s], loc.at[m]) for m in range(3)
+    ]
+    local.append(pltpu.make_async_copy(ow_hbm, ow_v, loc.at[3]))
+    local.append(pltpu.make_async_copy(
+        res_hbm.at[:, pl.ds(pl.multiple_of(t * C, C), C)], res_v, loc.at[4]))
+    for c in (local[3], local[4], local[0], local[1], local[2]):
+        c.start()
+
+    barrier = pltpu.get_barrier_semaphore()
+    peers = [(zp, t), (zm, t), (xp, t), (after_s, t), (before_s, t)]
+    peers += [(s, (t + d) % T) for d in range(1, T)]
+    for p in peers:
+        pl.semaphore_signal(barrier, inc=1, device_id=p, device_id_type=MESH)
+    pl.semaphore_wait(barrier, len(peers))
+
+    started = []
+
+    tails = []
+    for i, (a, b) in enumerate((
+        (k_ref.at[pl.ds(R - WINDOW, WINDOW)], kx.at[pl.ds(0, WINDOW)]),
+        (v_ref.at[pl.ds(R - WINDOW, WINDOW)], vx.at[pl.ds(0, WINDOW)]),
+        (doc_ref.at[pl.ds(doc_ref.shape[0] - 8, 8)], dx.at[pl.ds(0, 8)]),
+    )):
+        c = pltpu.make_async_remote_copy(
+            src_ref=a, dst_ref=b, send_sem=tail_send.at[i], recv_sem=tail_recv.at[i],
+            device_id=(after_s, t), device_id_type=MESH)
+        c.start()
+        tails.append(c)
+
+    target = (zp, zm, xp)
+    count = [0, 0, 0]
+
+    def send(link, m, src, h, own=False):
+        part = pl.ds(h * HK, HK)
+        place = G.at[m, src, part]
+        c = pltpu.make_async_remote_copy(
+            src_ref=weights[m].at[part] if own else place, dst_ref=place,
+            send_sem=w_send.at[link, count[link]], recv_sem=w_recv.at[m, src, h],
+            device_id=(target[link], t), device_id_type=MESH)
+        count[link] += 1
+        c.start()
+        started.append(c)
+
+    def recv(m, src, h):
+        place = G.at[m, src, pl.ds(h * HK, HK)]
+        pltpu.make_async_remote_copy(
+            src_ref=place, dst_ref=place, send_sem=w_send.at[0, 0],
+            recv_sem=w_recv.at[m, src, h], device_id=(zp, t), device_id_type=MESH).wait_recv()
+
+    for m in (0, 1):
+        for h in (0, 1):
+            for link in (0, 1, 2):
+                send(link, m, s, h, own=True)
+
+    kx[pl.ds(WINDOW, R), :] = k_ref[...]
+    vx[pl.ds(WINDOW, R), :] = v_ref[...]
+    dx[pl.ds(8, doc_ref.shape[0]), :] = doc_ref[...]
+    for c in tails:
+        c.wait_recv()
+    heads = q_ref.shape[1] // HEAD_DIM
+
+    def block(b, carry):
+        rows = pl.ds(pl.multiple_of(b * WINDOW, WINDOW), WINDOW)
+        band = pl.ds(pl.multiple_of(b * WINDOW, WINDOW), 2 * WINDOW)
+        prev = dx[pl.ds(pl.multiple_of(b * 8, 8), 8), :][0:1].astype(jnp.float32)
+        own = dx[pl.ds(pl.multiple_of(b * 8 + 8, 8), 8), :][0:1].astype(jnp.float32)
+        doc_q = jnp.broadcast_to(own, (WINDOW, WINDOW)).T
+        i = lax.broadcasted_iota(jnp.int32, (WINDOW, WINDOW), 0)
+        j = lax.broadcasted_iota(jnp.int32, (WINDOW, WINDOW), 1)
+        first = s * R + b * WINDOW - WINDOW
+        see_prev = (j > i) & (doc_q == prev) & (first + j >= 0)
+        see_own = (j <= i) & (doc_q == own)
+        visible = jnp.concatenate(
+            [see_prev.astype(jnp.float32), see_own.astype(jnp.float32)], axis=1) > 0.5
+        for h in range(heads):
+            kv = h // GROUP
+            cols = slice(kv * HEAD_DIM, (kv + 1) * HEAD_DIM)
+            q = q_ref[rows, h * HEAD_DIM:(h + 1) * HEAD_DIM]
+            scores = dot(q, kx[band, cols], NT) * HEAD_DIM ** (-0.5)
+            scores = jnp.where(visible, scores, neg_big)
+            sink = sink_ref[h]
+            row_max = jnp.maximum(scores.max(-1, keepdims=True), sink)
+            expo = jnp.where(visible, jnp.exp(scores - row_max), 0.0)
+            total = expo.sum(-1, keepdims=True) + jnp.exp(sink - row_max)
+            w = (expo / total).astype(jnp.bfloat16)
+            att[rows, h * HEAD_DIM:(h + 1) * HEAD_DIM] = dot(w, vx[band, cols]).astype(jnp.bfloat16)
+        return carry
+
+    lax.fori_loop(0, R // WINDOW, block, 0)
+
+    local[3].wait()
+    reach = [(t + d) % T for d in (2, 1, 3)]
+    psent = []
+    for n, owner in enumerate(reach + [t]):
+        cols = pl.ds(pl.multiple_of(owner * C, C), C)
+        value = dot(att[...], ow_v[:, cols]).astype(jnp.bfloat16)
+        if n == T - 1:
+            precv[t] = value
+        else:
+            psend[owner] = value
+            c = pltpu.make_async_remote_copy(
+                src_ref=psend.at[owner], dst_ref=precv.at[t], send_sem=p_send.at[n],
+                recv_sem=p_recv.at[t], device_id=(s, owner), device_id_type=MESH)
+            c.start()
+            psent.append(c)
+
+    def recv_block(buf, sems, source):
+        pltpu.make_async_remote_copy(
+            src_ref=buf.at[source], dst_ref=buf.at[source], send_sem=p_send.at[0],
+            recv_sem=sems.at[source], device_id=(s, (t + 1) % T), device_id_type=MESH).wait_recv()
+
+    recv(0, zm, 0)
+    send(0, 0, zm, 0)
+    recv(0, zp, 1)
+    send(1, 0, zp, 1)
+    recv(0, zm, 1)
+    recv(0, zp, 0)
+    send(2, 0, zm, 1)
+    send(2, 0, zp, 1)
+    recv(1, zm, 0)
+    send(0, 1, zm, 0)
+    recv(1, zp, 1)
+    send(1, 1, zp, 1)
+    recv(1, zm, 1)
+    recv(1, zp, 0)
+    recv(0, xp, 0)
+    recv(0, xp, 1)
+    recv(1, xp, 0)
+    recv(1, xp, 1)
+    for m, h in ((0, 0), (1, 0), (1, 1)):
+        send(0, m, xp, h)
+        send(1, m, xp, h)
+    send(0, 2, s, 0, own=True)
+    send(0, 2, s, 1, own=True)
+    send(1, 2, s, 1, own=True)
+    send(1, 2, s, 0, own=True)
+
+    local[4].wait()
+    for owner in reach:
+        recv_block(precv, p_recv, owner)
+    total = precv[0].astype(jnp.float32)
+    for i in range(1, T):
+        total += precv[i].astype(jnp.float32)
+    after[t] = (res_v[...].astype(jnp.float32) + total).astype(jnp.bfloat16)
+    asent = []
+    for n, peer in enumerate(reach):
+        c = pltpu.make_async_remote_copy(
+            src_ref=after.at[t], dst_ref=after.at[t], send_sem=a_send.at[n],
+            recv_sem=a_recv.at[t], device_id=(s, peer), device_id_type=MESH)
+        c.start()
+        asent.append(c)
+
+    for m in (0, 1):
+        for h in (0, 1):
+            recv(m, z2, h)
+            send(2, m, z2, h)
+    send(2, 2, s, 0, own=True)
+    send(2, 2, s, 1, own=True)
+
+    for peer in reach:
+        recv_block(after, a_recv, peer)
+
+    def norm(r, carry):
+        rows = pl.ds(pl.multiple_of(r * 64, 64), 64)
+        parts = [after[i, rows, :].astype(jnp.float32) for i in range(T)]
+        square = (parts[0] * parts[0]).sum(-1, keepdims=True)
+        for p in parts[1:]:
+            square += (p * p).sum(-1, keepdims=True)
+        inv = lax.rsqrt(square / D + norm_eps)
+        for i in range(T):
+            n = (parts[i] * inv * gain_ref[:, i * C:(i + 1) * C]).astype(jnp.bfloat16)
+            for j in range(PER):
+                normed[i * PER + j, rows, :] = n[:, j * K:(j + 1) * K]
+        return carry
+
+    lax.fori_loop(0, R // 64, norm, 0)
+
+    TM = 128
+
+    def gate_up(src, begin=False):
+        def tile(r, carry):
+            rows = pl.ds(pl.multiple_of(r * TM, TM), TM)
+            a = normed[src, rows, :]
+            for m, acc in ((0, ga), (1, ua)):
+                value = dot(a, G[m, src])
+                if begin:
+                    acc[rows, :] = value
+                else:
+                    acc[rows, :] += value
+            return carry
+        lax.fori_loop(0, R // TM, tile, 0)
+
+    local[0].wait()
+    local[1].wait()
+    gate_up(s, True)
+    for src in (zm, zp, xp, z2):
+        gate_up(src)
+    for src in (zm_x, zp_x):
+        for m in (0, 1):
+            for h in (0, 1):
+                recv(m, src, h)
+        gate_up(src)
+    recv(2, zm, 0)
+    send(0, 2, zm, 0)
+    recv(2, zp, 1)
+    send(1, 2, zp, 1)
+    for m in (0, 1):
+        for h in (0, 1):
+            recv(m, z2_x, h)
+    gate_up(z2_x)
+
+    def act(r, carry):
+        rows = pl.ds(pl.multiple_of(r * 32, 32), 32)
+        g = ga[rows, :]
+        hidden[rows, :] = (g / (1.0 + jnp.exp(-g)) * ua[rows, :]).astype(jnp.bfloat16)
+        return carry
+
+    lax.fori_loop(0, R // 32, act, 0)
+
+    def down_copy(src, h):
+        owner = src // PER
+        return owner, pltpu.make_async_remote_copy(
+            src_ref=dsend.at[src, h], dst_ref=drecv.at[t, src % PER, h],
+            send_sem=d_send.at[src, h], recv_sem=d_recv.at[t, src % PER, h],
+            device_id=(s, owner), device_id_type=MESH)
+
+    def down(src, h):
+        value = dot(hidden[...], G[2, src, h * HK:(h + 1) * HK, :], NT).astype(jnp.bfloat16)
+        owner, c = down_copy(src, h)
+
+        @pl.when(owner != t)
+        def _():
+            dsend[src, h] = value
+            c.start()
+
+        @pl.when(owner == t)
+        def _():
+            drecv[t, src % PER, h] = value
+
+    local[2].wait()
+    for h in (0, 1):
+        recv(2, xp, h)
+        send(0, 2, xp, h)
+        send(1, 2, xp, h)
+        recv(2, z2, h)
+        send(2, 2, z2, h)
+        if h == 0:
+            down(s, 0)
+            down(s, 1)
+    recv(2, zm, 1)
+    recv(2, zp, 0)
+    for src in (zm, zp, xp, z2):
+        for h in (0, 1):
+            down(src, h)
+    for h in (0, 1):
+        for src in (zm_x, zp_x, z2_x):
+            recv(2, src, h)
+            down(src, h)
+
+    for i in range(PER):
+        for h in (0, 1):
+            for peer in reach:
+                pltpu.make_async_remote_copy(
+                    src_ref=drecv.at[peer, i, h], dst_ref=drecv.at[peer, i, h],
+                    send_sem=d_send.at[0, 0], recv_sem=d_recv.at[peer, i, h],
+                    device_id=(s, (t + 1) % T), device_id_type=MESH).wait_recv()
+            total = drecv[0, i, h].astype(jnp.float32)
+            for n in range(1, T):
+                total += drecv[n, i, h].astype(jnp.float32)
+            cols = slice((i * 2 + h) * HK, (i * 2 + h + 1) * HK)
+            out_ref[:, cols] = (after[t, :, cols].astype(jnp.float32) + total).astype(jnp.bfloat16)
+
+    for c in started + tails + psent + asent:
+        c.wait_send()
+    for src in range(S):
+        for h in (0, 1):
+            owner, c = down_copy(src, h)
+
+            @pl.when(owner != t)
+            def _():
+                c.wait_send()
+
+
+def fused(residual, queries, keys, values, documents, sinks, out_weight, norm_gain, gate_weight, up_weight, down_weight):
+    S, T = lax.axis_size("sp"), lax.axis_size("tp")
+    R, D = residual.shape
+    F = gate_weight.shape[1]
+    C, K = D // T, D // S
+    blocks = R // WINDOW
+    docs = jnp.broadcast_to(documents.reshape(blocks, 1, WINDOW), (blocks, 8, WINDOW)).reshape(blocks * 8, WINDOW)
+    bf, f32 = jnp.bfloat16, jnp.float32
+    vm, hbm = pl.BlockSpec(memory_space=pltpu.VMEM), pl.BlockSpec(memory_space=pl.ANY)
+    dma = pltpu.SemaphoreType.DMA
+    scratch = [
+        pltpu.VMEM((3, S, K, F), bf),
+        pltpu.VMEM((R + WINDOW, keys.shape[1]), bf),
+        pltpu.VMEM((R + WINDOW, keys.shape[1]), bf),
+        pltpu.VMEM((blocks * 8 + 8, WINDOW), jnp.int32),
+        pltpu.VMEM((R, queries.shape[1]), bf),
+        pltpu.VMEM((R, C), bf),
+        pltpu.VMEM(out_weight.shape, bf),
+        pltpu.VMEM((T, R, C), bf),
+        pltpu.VMEM((T, R, C), bf),
+        pltpu.VMEM((T, R, C), bf),
+        pltpu.VMEM((S, R, K), bf),
+        pltpu.VMEM((R, F), f32),
+        pltpu.VMEM((R, F), f32),
+        pltpu.VMEM((R, F), bf),
+        pltpu.VMEM((S, 2, R, K // 2), bf),
+        pltpu.VMEM((T, C // K, 2, R, K // 2), bf),
+        dma((3, 14)), dma((3, S, 2)), dma((3,)), dma((3,)), dma((5,)),
+        dma((T,)), dma((T,)), dma((T,)), dma((T,)), dma((S, 2)), dma((T, C // K, 2)),
+    ]
+    return pl.pallas_call(
+        functools.partial(kernel, S, T),
+        out_shape=jax.ShapeDtypeStruct((R, C), bf),
+        in_specs=[hbm, vm, vm, vm, vm, pl.BlockSpec(memory_space=pltpu.SMEM), hbm, vm, hbm, hbm, hbm],
+        out_specs=vm,
+        scratch_shapes=scratch,
+        compiler_params=pltpu.CompilerParams(
+            collective_id=0, has_side_effects=True, vmem_limit_bytes=60 * 2**20),
+    )(residual, queries, keys, values, docs, sinks, out_weight, norm_gain.reshape(1, D),
+      gate_weight, up_weight, down_weight)
+
+
+def ring_of_four_pairs(mesh):
+    return mesh.shape["sp"] == 8 and mesh.shape["tp"] == 4
+
+
 def solution(mesh):
     return jax.shard_map(
-        on_device,
+        fused if ring_of_four_pairs(mesh) else on_device,
         mesh=mesh,
         in_specs=(
             P("sp", None),

time: 368 us -> 237 us (0.64)
  waiting for transfers between devices: 296 us -> 0 us
  Pallas kernels: 0 us -> 230 us
  matrix products: 25.5 us -> 0 us
  between operations: 15.2 us -> 0.01 us
  starting transfers between devices: 12.7 us -> 0 us
  other arithmetic: 7.52 us -> 0 us
  local copies, waits for them, and re-layouts: 10.2 us -> 3.16 us
    pallas_call x0 -> x1, Pallas kernels: none -> 230 us  [fused(): pl.pallas_call(functools.partial(kernel, S, T), out_shape=jax.ShapeDtypeS...]
    all_gather x3 -> x0, waiting for transfers between devices: 217 us -> none  [the longest x1 92.4 us: on_device(): down_full = lax.all_gather(down_weight, 'sp', axis=0, tiled=True)]
    psum x1 -> x0, waiting for transfers between devices: 48.3 us -> none  [on_device(): lax.psum(full_term.astype(jnp.bfloat16), 'tp').astype(jnp.float32)]
    reduce_scatter x1 -> x0, waiting for transfers between devices: 29.5 us -> none  [on_device(): lax.psum_scatter(lax.dot_general(down_full, hidden, (((1,), (1,)), ((), (...]
    dot_general x5 -> x0, matrix products: 25.5 us -> none  [the longest x1 13.4 us: on_device(): lax.dot_general(down_full, hidden, (((1,), (1,)), ((), ())), preferred_el...]
    ppermute x3 -> x0, starting transfers between devices: 12.3 us -> none  [from_behind(): return lax.ppermute(shard, axis, pairs)]
    slice x12 -> x0, local copies, waits for them, and re-layouts: 3.93 us -> none  [the longest x1 1.36 us: on_device(): values[rows_here - WINDOW:]]
    reshape x5 -> x1, local copies, waits for them, and re-layouts: 4.37 us -> 0.61 us  [fused(): jnp.broadcast_to(documents.reshape(blocks, 1, WINDOW), (blocks, 8, WINDOW))]
  transfers between devices with their start and end apart: 8 -> 0, of which waited for: 5 -> 0; matrix products, arithmetic and copies ran while one was open for 6% -> 0% of each run, Pallas kernels for 0% -> 0%
where the time goes in v1:
time: 237 us; the launch traced here: 233 us
  Pallas kernels  230 us (97%)
  local copies, waits for them, and re-layouts  3.16 us (1%)
    pallas_call x1, Pallas kernels, fused(): pl.pallas_call(functools.partial(kernel, S, T), out_shape=jax.ShapeDtypeS...  230 us

profile of v1, /device:TPU:0, one launch (start us, length us, event | category | flops | bytes accessed | tf_op | source)
XLA Modules:
  0.0 232.9 jit_solution(7292058301681136077)
XLA Ops:
  0.0 0.0 copy-start
  0.0 0.7 copy-done
  0.7 0.6 broadcast_bitcast_fusion.doc_ref
  1.3 229.8 %shard_map.109 = bf16[512,512]{1,0:T(8,128)(2,1)} custom-call(bf16[512,2048]{1,0:T(8,128)(2,1)} %res_hbm.1, bf16[512,256]{1,0:T(8,128)(2,1)} %q_ref.1, bf16[512,128]{1,0:T(8,128)(2,1)} %k_ref.1, bf16[512,128]{1,0:T(8,128)(2,1)} %v_ref.1, s32[32,128]{1,0:T(8,128)} %broadcast_bitcast_fusion.doc_ref, f32[4]{0:T(128)} %sink_ref.1, bf16[256,2048]{1,0:T(8,128)(2,1)} %ow_hbm.1, ...), custom_call_target="tpu_custom_call" | custom-call | tf_op jit(solution)/shard_map/pallas_call | solution.py:475
  231.1 1.9 copy.13
Async XLA Ops:
  0.0 0.7 copy-start

commit v2 on v1

--- a/solution.py
+++ b/solution.py
@@ -147,13 +147,16 @@
     HK = K // 2
     PER = C // K
     z, x = s // 2, s % 2
-    zp = ((z + 1) % 4) * 2 + x
-    zm = ((z + 3) % 4) * 2 + x
-    z2 = ((z + 2) % 4) * 2 + x
-    xp = z * 2 + (1 - x)
-    zp_x = ((z + 1) % 4) * 2 + (1 - x)
-    zm_x = ((z + 3) % 4) * 2 + (1 - x)
-    z2_x = ((z + 2) % 4) * 2 + (1 - x)
+    up, down_z = (z + 1) % 4, (z + 3) % 4
+    nb_z = z + 1 - 2 * (z % 2)
+    f1_z = 2 - z // 2
+    f2_z = 3 - 3 * (z // 2)
+    zp, zm, xp = up * 2 + x, down_z * 2 + x, z * 2 + 1 - x
+    nb, f1, f2 = nb_z * 2 + x, f1_z * 2 + x, f2_z * 2 + x
+    nb_x, f1_x, f2_x = nb_z * 2 + 1 - x, f1_z * 2 + 1 - x, f2_z * 2 + 1 - x
+    far = ((z + 2) % 4) * 2 + x
+    end = (3 - z) * 2 + x
+    has_up, has_down = z < 3, z > 0
     after_s = (s + 1) % S
     before_s = (s + S - 1) % S
 
@@ -188,10 +191,16 @@
         c.start()
         tails.append(c)
 
-    target = (zp, zm, xp)
-    count = [0, 0, 0]
-
-    def send(link, m, src, h, own=False):
+    target = (zp, zm, xp, nb)
+    count = [0, 0, 0, 0]
+
+    def when(cond, f):
+        if cond is None:
+            f()
+        else:
+            pl.when(cond)(f)
+
+    def send(link, m, src, h, own=False, cond=None):
         part = pl.ds(h * HK, HK)
         place = G.at[m, src, part]
         c = pltpu.make_async_remote_copy(
@@ -199,19 +208,59 @@
             send_sem=w_send.at[link, count[link]], recv_sem=w_recv.at[m, src, h],
             device_id=(target[link], t), device_id_type=MESH)
         count[link] += 1
-        c.start()
-        started.append(c)
-
-    def recv(m, src, h):
+        when(cond, c.start)
+        started.append((cond, c))
+
+    def recv(m, src, h, cond=None):
         place = G.at[m, src, pl.ds(h * HK, HK)]
-        pltpu.make_async_remote_copy(
+        c = pltpu.make_async_remote_copy(
             src_ref=place, dst_ref=place, send_sem=w_send.at[0, 0],
-            recv_sem=w_recv.at[m, src, h], device_id=(zp, t), device_id_type=MESH).wait_recv()
-
-    for m in (0, 1):
-        for h in (0, 1):
-            for link in (0, 1, 2):
-                send(link, m, s, h, own=True)
+            recv_sem=w_recv.at[m, src, h], device_id=(xp, t), device_id_type=MESH)
+        when(cond, c.wait_recv)
+
+    GU = ((0, 0), (0, 1), (1, 0), (1, 1))
+    DN = ((2, 0), (2, 1))
+
+    def own_z(units):
+        for m, h in units:
+            send(0, m, s, h, own=True, cond=has_up)
+            send(1, m, s, h, own=True, cond=has_down)
+
+    def own_x(units):
+        for m, h in units:
+            send(2, m, s, h, own=True)
+
+    def near(units):
+        for m, h in units:
+            recv(m, zp, h, has_up)
+            send(1, m, zp, h, cond=has_up & has_down)
+            recv(m, zm, h, has_down)
+            send(0, m, zm, h, cond=has_up & has_down)
+            if h == 1:
+                send(2, m, nb, h)
+
+    def middle(units):
+        for m, h in units:
+            recv(m, far, h)
+            send(1, m, far, h, cond=z == 1)
+            send(0, m, far, h, cond=z == 2)
+            send(2, m, f1, h)
+
+    def farthest(units):
+        for m, h in units:
+            recv(m, end, h, (z == 0) | (z == 3))
+            send(2, m, f2, h)
+
+    def extra(units):
+        for m, h in units:
+            recv(m, xp, h)
+            if h == 0:
+                send(3, m, xp, h)
+
+    for m, h in GU:
+        send(0, m, s, h, own=True, cond=has_up)
+        send(1, m, s, h, own=True, cond=has_down)
+        send(2, m, s, h, own=True)
 
     kx[pl.ds(WINDOW, R), :] = k_ref[...]
     vx[pl.ds(WINDOW, R), :] = v_ref[...]
@@ -270,31 +319,7 @@
             src_ref=buf.at[source], dst_ref=buf.at[source], send_sem=p_send.at[0],
             recv_sem=sems.at[source], device_id=(s, (t + 1) % T), device_id_type=MESH).wait_recv()
 
-    recv(0, zm, 0)
-    send(0, 0, zm, 0)
-    recv(0, zp, 1)
-    send(1, 0, zp, 1)
-    recv(0, zm, 1)
-    recv(0, zp, 0)
-    send(2, 0, zm, 1)
-    send(2, 0, zp, 1)
-    recv(1, zm, 0)
-    send(0, 1, zm, 0)
-    recv(1, zp, 1)
-    send(1, 1, zp, 1)
-    recv(1, zm, 1)
-    recv(1, zp, 0)
-    recv(0, xp, 0)
-    recv(0, xp, 1)
-    recv(1, xp, 0)
-    recv(1, xp, 1)
-    for m, h in ((0, 0), (1, 0), (1, 1)):
-        send(0, m, xp, h)
-        send(1, m, xp, h)
-    send(0, 2, s, 0, own=True)
-    send(0, 2, s, 1, own=True)
-    send(1, 2, s, 1, own=True)
-    send(1, 2, s, 0, own=True)
+    near(GU)
 
     local[4].wait()
     for owner in reach:
@@ -311,12 +336,9 @@
         c.start()
         asent.append(c)
 
-    for m in (0, 1):
-        for h in (0, 1):
-            recv(m, z2, h)
-            send(2, m, z2, h)
-    send(2, 2, s, 0, own=True)
-    send(2, 2, s, 1, own=True)
+    middle(GU)
+    extra(GU)
+    own_z(DN)
 
     for peer in reach:
         recv_block(after, a_recv, peer)
@@ -354,21 +376,17 @@
     local[0].wait()
     local[1].wait()
     gate_up(s, True)
-    for src in (zm, zp, xp, z2):
+    gate_up(nb)
+    farthest(GU[:2])
+    gate_up(xp)
+    gate_up(f1)
+    farthest(GU[2:])
+    own_x(DN)
+    gate_up(f2)
+    for src in (nb_x, f1_x, f2_x):
+        for m, h in GU:
+            recv(m, src, h)
         gate_up(src)
-    for src in (zm_x, zp_x):
-        for m in (0, 1):
-            for h in (0, 1):
-                recv(m, src, h)
-        gate_up(src)
-    recv(2, zm, 0)
-    send(0, 2, zm, 0)
-    recv(2, zp, 1)
-    send(1, 2, zp, 1)
-    for m in (0, 1):
-        for h in (0, 1):
-            recv(m, z2_x, h)
-    gate_up(z2_x)
 
     def act(r, carry):
         rows = pl.ds(pl.multiple_of(r * 32, 32), 32)
@@ -399,23 +417,25 @@
             drecv[t, src % PER, h] = value
 
     local[2].wait()
-    for h in (0, 1):
-        recv(2, xp, h)
-        send(0, 2, xp, h)
-        send(1, 2, xp, h)
-        recv(2, z2, h)
-        send(2, 2, z2, h)
-        if h == 0:
-            down(s, 0)
-            down(s, 1)
-    recv(2, zm, 1)
-    recv(2, zp, 0)
-    for src in (zm, zp, xp, z2):
+    near(DN)
+    down(s, 0)
+    down(s, 1)
+    down(nb, 0)
+    down(nb, 1)
+    middle(DN)
+    extra(DN)
+    for src in (xp, f1):
         for h in (0, 1):
             down(src, h)
-    for h in (0, 1):
-        for src in (zm_x, zp_x, z2_x):
-            recv(2, src, h)
+    for h in (1, 0):
+        if h == 0:
+            farthest(DN)
+        recv(2, nb_x, h)
+        down(nb_x, h)
+    for src in (f2, f1_x, f2_x):
+        for h in (0, 1):
+            if src is not f2:
+                recv(2, src, h)
             down(src, h)
 
     for i in range(PER):
@@ -431,7 +451,9 @@
             cols = slice((i * 2 + h) * HK, (i * 2 + h + 1) * HK)
             out_ref[:, cols] = (after[t, :, cols].astype(jnp.float32) + total).astype(jnp.bfloat16)
 
-    for c in started + tails + psent + asent:
+    for cond, c in started:
+        when(cond, c.wait_send)
+    for c in tails + psent + asent:
         c.wait_send()
     for src in range(S):
         for h in (0, 1):
@@ -469,7 +491,7 @@
         pltpu.VMEM((R, F), bf),
         pltpu.VMEM((S, 2, R, K // 2), bf),
         pltpu.VMEM((T, C // K, 2, R, K // 2), bf),
-        dma((3, 14)), dma((3, S, 2)), dma((3,)), dma((3,)), dma((5,)),
+        dma((4, 21)), dma((3, S, 2)), dma((3,)), dma((3,)), dma((5,)),
         dma((T,)), dma((T,)), dma((T,)), dma((T,)), dma((S, 2)), dma((T, C // K, 2)),
     ]
     return pl.pallas_call(
@@ -484,13 +506,13 @@
       gate_weight, up_weight, down_weight)
 
 
-def ring_of_four_pairs(mesh):
+def line_of_four_pairs(mesh):
     return mesh.shape["sp"] == 8 and mesh.shape["tp"] == 4
 
 
 def solution(mesh):
     return jax.shard_map(
-        fused if ring_of_four_pairs(mesh) else on_device,
+        fused if line_of_four_pairs(mesh) else on_device,
         mesh=mesh,
         in_specs=(
             P("sp", None),

time: 237 us -> 195 us (0.82)
  Pallas kernels: 230 us -> 190 us
    pallas_call x1, Pallas kernels: 230 us -> 190 us  [fused(): pl.pallas_call(functools.partial(kernel, S, T), out_shape=jax.ShapeDtypeS...]
where the time goes in v2:
time: 195 us; the launch traced here: 193 us
  Pallas kernels  190 us (97%)
  local copies, waits for them, and re-layouts  3.16 us (2%)
    pallas_call x1, Pallas kernels, fused(): pl.pallas_call(functools.partial(kernel, S, T), out_shape=jax.ShapeDtypeS...  190 us

profile of v2, /device:TPU:0, one launch (start us, length us, event | category | flops | bytes accessed | tf_op | source)
XLA Modules:
  0.0 193.3 jit_solution(11646042336545049053)
XLA Ops:
  0.0 0.0 copy-start
  0.0 0.7 copy-done
  0.7 0.6 broadcast_bitcast_fusion.doc_ref
  1.3 190.1 %shard_map.109 = bf16[512,512]{1,0:T(8,128)(2,1)} custom-call(bf16[512,2048]{1,0:T(8,128)(2,1)} %res_hbm.1, bf16[512,256]{1,0:T(8,128)(2,1)} %q_ref.1, bf16[512,128]{1,0:T(8,128)(2,1)} %k_ref.1, bf16[512,128]{1,0:T(8,128)(2,1)} %v_ref.1, s32[32,128]{1,0:T(8,128)} %broadcast_bitcast_fusion.doc_ref, f32[4]{0:T(128)} %sink_ref.1, bf16[256,2048]{1,0:T(8,128)(2,1)} %ow_hbm.1, ...), custom_call_target="tpu_custom_call" | custom-call | tf_op jit(solution)/shard_map/pallas_call | solution.py:497
  191.4 1.9 copy.13
Async XLA Ops:
  0.0 0.7 copy-start

commit v3 on v2

--- a/solution.py
+++ b/solution.py
@@ -339,6 +339,7 @@
     middle(GU)
     extra(GU)
     own_z(DN)
+    farthest(GU[:2])
 
     for peer in reach:
         recv_block(after, a_recv, peer)
@@ -377,11 +378,10 @@
     local[1].wait()
     gate_up(s, True)
     gate_up(nb)
-    farthest(GU[:2])
+    farthest(GU[2:])
+    own_x(DN)
     gate_up(xp)
     gate_up(f1)
-    farthest(GU[2:])
-    own_x(DN)
     gate_up(f2)
     for src in (nb_x, f1_x, f2_x):
         for m, h in GU:

time: 195 us -> 195 us (level)
  no operation moved by 1% of the time
where the time goes in v3:
time: 195 us; the launch traced here: 193 us
  Pallas kernels  190 us (97%)
  local copies, waits for them, and re-layouts  3.16 us (2%)
    pallas_call x1, Pallas kernels, fused(): pl.pallas_call(functools.partial(kernel, S, T), out_shape=jax.ShapeDtypeS...  190 us

profile of v3, /device:TPU:0, one launch (start us, length us, event | category | flops | bytes accessed | tf_op | source)
XLA Modules:
  0.0 193.3 jit_solution(16332426959118643296)
XLA Ops:
  0.0 0.0 copy-start
  0.0 0.7 copy-done
  0.7 0.6 broadcast_bitcast_fusion.doc_ref
  1.3 190.1 %shard_map.109 = bf16[512,512]{1,0:T(8,128)(2,1)} custom-call(bf16[512,2048]{1,0:T(8,128)(2,1)} %res_hbm.1, bf16[512,256]{1,0:T(8,128)(2,1)} %q_ref.1, bf16[512,128]{1,0:T(8,128)(2,1)} %k_ref.1, bf16[512,128]{1,0:T(8,128)(2,1)} %v_ref.1, s32[32,128]{1,0:T(8,128)} %broadcast_bitcast_fusion.doc_ref, f32[4]{0:T(128)} %sink_ref.1, bf16[256,2048]{1,0:T(8,128)(2,1)} %ow_hbm.1, ...), custom_call_target="tpu_custom_call" | custom-call | tf_op jit(solution)/shard_map/pallas_call | solution.py:497
  191.4 1.9 copy.13
Async XLA Ops:
  0.0 0.7 copy-start
